TPU v7x, 32 devices: a whole 2x2x4 slice. The times are simulated.
32 devices in a mesh: ep: 8 (over z, x), tp: 4 (over y, core).
Axes of the slice: x: 2, y: 2, z: 4, core: 2. Of those that a mesh axis runs over, the one named last changes fastest.
Arguments:
- queries: bfloat16 [2048, 2048], P('ep', 'tp'), may hold values from -9 to 9
- key_rows: bfloat16 [2048, 2048], P('ep', 'tp'), may hold values from -9 to 9
- values: bfloat16 [2048, 2048], P('ep', 'tp'), may hold values from -6 to 6
- second_scale: float32 [16], P('tp'), may hold values from 0.3 to 0.8
- head_gain: float32 [128], replicated, may hold values from 0.1 to 1.9
- out_weight: bfloat16 [2048, 2048], P(None, 'tp'), may hold values from -0.125 to 0.125
- routed_in: bfloat16 [2048, 2048], P('ep'), may hold values from -6 to 6
- routed_gain: float32 [2048], replicated, may hold values from 0.1 to 1.9
- expert_ids: int32 [2048, 2], P('ep'), may hold values from 0 to 7, all different within a row; in each aligned block of 256 rows (0 to 255, 256 to 511, ...) at most 128 rows name the same one
- group_logits: float32 [2048, 2], P('ep'), may hold values from -6 to 6
- inner_logits: float32 [2048, 2], P('ep'), may hold values from -6 to 6
- gate_weight: bfloat16 [8, 2048, 4096], P('ep', None, 'tp'), may hold values from -0.125 to 0.125
- up_weight: bfloat16 [8, 2048, 4096], P('ep', None, 'tp'), may hold values from -0.125 to 0.125
- down_weight: bfloat16 [8, 4096, 2048], P('ep', 'tp'), may hold values from -0.09375 to 0.09375
Outputs:
- mixer_out: bfloat16 [2048, 2048], P('ep', 'tp')
- routed_out: bfloat16 [2048, 2048], P('ep', 'tp')
Inputs may be any that keep to these rules, and one draw needn't show every extreme that they name: `expert_ids`: the two ids of a row differ. In the rows of one device (aligned blocks of 256 rows) no expert is named by more than 128 rows, a bound that some block reaches.
All inputs are finite; a program needn't handle non-finite values.
Results may differ from a plain program's by a relative error of at most 0.018.
Values may be sent and summed in bfloat16 or wider, within the bound.
No kernel may reach another device: no remote copies, remote signals or barrier semaphores. Data moves between devices by JAX's collectives and lax.ppermute only.
A program may use at most 128 MiB of HBM per device.

v0:
```python
import math
import jax
import jax.numpy as jnp
from jax import lax
from jax.sharding import PartitionSpec as P

GROUP_SIZE = 4
EPSILON = 1e-05
LOWEST = -1e30


def token_mixer(queries, key_rows, values, second_scale, head_gain, out_weight):
    row_count = queries.shape[0]
    local_heads = second_scale.shape[0]
    qk_size = queries.shape[1] // (2 * local_heads)
    value_size = values.shape[1] // local_heads
    first_pos = lax.axis_index("ep") * row_count
    query_pos = first_pos + jnp.arange(row_count, dtype=jnp.int32)
    last_pos = first_pos + row_count - 1
    query_four = queries.reshape(row_count, local_heads, 2, qk_size)
    score_scale = qk_size ** (-0.5)
    initial = (
        jnp.full((row_count, local_heads, 2), LOWEST, jnp.float32),
        jnp.zeros((row_count, local_heads, 2), jnp.float32),
        jnp.zeros((row_count, local_heads, 2, value_size), jnp.float32),
    )
    state_now = initial
    key_piece = lax.all_gather(key_rows, "ep", axis=0, tiled=True)
    value_piece = lax.all_gather(values, "ep", axis=0, tiled=True)
    piece_count = key_piece.shape[0]
    block_width = math.gcd(piece_count, 512)
    blocks = piece_count // block_width
    key_blocks = key_piece.reshape(blocks, block_width, local_heads, 2, qk_size)
    value_blocks = value_piece.reshape(blocks, block_width, local_heads, value_size)

    def update(state_inner, block_index):
        key_start = block_index * block_width

        def attend(inner_state):
            running_max, denominator, weighted = inner_state
            scores = (
                jnp.einsum(
                    "qhmd,khmd->qhmk",
                    query_four,
                    key_blocks[block_index],
                    preferred_element_type=jnp.float32,
                )
                * score_scale
            )
            key_pos = key_start + jnp.arange(block_width, dtype=jnp.int32)
            visible = (query_pos[:, None] >= key_pos[None, :])[:, None, None, :]
            scores = jnp.where(visible, scores, LOWEST)
            new_max = jnp.maximum(running_max, jnp.max(scores, axis=-1))
            exp_terms = jnp.where(visible, jnp.exp(scores - new_max[..., None]), 0.0)
            factor = jnp.exp(running_max - new_max)
            denominator = denominator * factor + jnp.sum(exp_terms, axis=-1)
            weighted = weighted * factor[..., None] + jnp.einsum(
                "qhmk,khe->qhme",
                exp_terms.astype(jnp.bfloat16),
                value_blocks[block_index],
                preferred_element_type=jnp.float32,
            )
            return (new_max, denominator, weighted)

        return (
            lax.cond(key_start <= last_pos, attend, lambda inner_state: inner_state, state_inner),
            None,
        )

    state_now, _ = lax.scan(update, state_now, jnp.arange(blocks, dtype=jnp.int32))
    running_max, denominator, weighted = state_now
    mapped = weighted / denominator[..., None]
    difference = mapped[:, :, 0] - second_scale[None, :, None] * mapped[:, :, 1]
    inv_norm = lax.rsqrt(jnp.mean(difference * difference, axis=-1, keepdims=True) + EPSILON)
    head_out = (
        (difference * inv_norm * head_gain)
        .astype(jnp.bfloat16)
        .reshape(row_count, local_heads * value_size)
    )
    mixed = jnp.dot(
        lax.all_gather(head_out, "tp", axis=1, tiled=True),
        out_weight,
        preferred_element_type=jnp.float32,
    )
    return mixed.astype(jnp.bfloat16)


def expert_block(
    routed_in,
    routed_gain,
    expert_ids,
    group_logits,
    inner_logits,
    gate_weight,
    up_weight,
    down_weight,
):
    token_count = routed_in.shape[0]
    chosen = expert_ids.shape[1]
    ep_size = lax.axis_size("ep")
    capacity = 2 * chosen * token_count // ep_size
    source = routed_in.astype(jnp.float32)
    normed = (
        source
        * lax.rsqrt(jnp.mean(source * source, axis=-1, keepdims=True) + EPSILON)
        * routed_gain
    ).astype(jnp.bfloat16)
    flat_ids = expert_ids.reshape(-1)
    picked = (flat_ids[:, None] == jnp.arange(ep_size, dtype=jnp.int32)[None, :]).astype(jnp.int32)
    slot_index = jnp.sum(jnp.cumsum(picked, axis=0) * picked, axis=1) - 1
    place_index = flat_ids * capacity + slot_index
    owner_row = jnp.arange(token_count * chosen, dtype=jnp.int32) // chosen
    slot_rows = jnp.zeros((ep_size * capacity,), jnp.int32).at[place_index].set(owner_row)
    outgoing = normed[slot_rows].reshape(ep_size, capacity, normed.shape[1])
    gate_local = gate_weight[0]
    up_local = up_weight[0]
    down_local = down_weight[0]
    columns = outgoing.shape[2] // lax.axis_size("tp")
    own_columns = lax.dynamic_slice_in_dim(outgoing, lax.axis_index("tp") * columns, columns, 2)
    arrived = lax.all_to_all(own_columns, "ep", split_axis=0, concat_axis=0, tiled=True)
    experts_arrived = lax.all_gather(arrived, "tp", axis=2, tiled=True)
    stacked = experts_arrived.reshape(-1, experts_arrived.shape[2])
    gate_act = jnp.dot(stacked, gate_local, preferred_element_type=jnp.float32)
    up_act = jnp.dot(stacked, up_local, preferred_element_type=jnp.float32)
    hidden = (jax.nn.silu(gate_act) * up_act).astype(jnp.bfloat16)
    partial_value = jnp.dot(hidden, down_local, preferred_element_type=jnp.float32)
    partial_value = partial_value.reshape(
        experts_arrived.shape[0], experts_arrived.shape[1], partial_value.shape[1]
    )
    answered = lax.psum_scatter(
        partial_value.astype(jnp.bfloat16), "tp", scatter_dimension=2, tiled=True
    )
    returned = lax.all_to_all(answered, "ep", split_axis=0, concat_axis=0, tiled=True)
    pair_out = returned.reshape(ep_size * capacity, returned.shape[2])[place_index]
    pair_out = pair_out.reshape(token_count, chosen, returned.shape[2])
    group_prob = jax.nn.softmax(group_logits, axis=-1)
    member = (
        expert_ids[..., None] // GROUP_SIZE == jnp.arange(group_logits.shape[1], dtype=jnp.int32)
    ).astype(jnp.float32)
    group_pick = jnp.sum(group_prob[:, None, :] * member, axis=-1)
    route_weight = group_pick * jax.nn.softmax(inner_logits, axis=-1)
    return jnp.sum(route_weight[..., None] * pair_out.astype(jnp.float32), axis=1).astype(
        jnp.bfloat16
    )


def local(
    queries,
    key_rows,
    values,
    second_scale,
    head_gain,
    out_weight,
    routed_in,
    routed_gain,
    expert_ids,
    group_logits,
    inner_logits,
    gate_weight,
    up_weight,
    down_weight,
):
    mixer_out = token_mixer(queries, key_rows, values, second_scale, head_gain, out_weight)
    routed_out = expert_block(
        routed_in,
        routed_gain,
        expert_ids,
        group_logits,
        inner_logits,
        gate_weight,
        up_weight,
        down_weight,
    )
    return (mixer_out, routed_out)


def solution(mesh):
    return jax.shard_map(
        local,
        mesh=mesh,
        in_specs=(
            P("ep", "tp"),
            P("ep", "tp"),
            P("ep", "tp"),
            P("tp"),
            P(),
            P(None, "tp"),
            P("ep", None),
            P(),
            P("ep", None),
            P("ep", None),
            P("ep", None),
            P("ep", None, "tp"),
            P("ep", None, "tp"),
            P("ep", "tp", None),
        ),
        out_specs=(P("ep", "tp"), P("ep", "tp")),
        check_vma=False,
    )
```

profile of v0, /device:TPU:0, one launch (start us, length us, event | category | flops | bytes accessed | tf_op | source)
XLA Modules:
  0.0 282.8 jit_solution(2242656608701986712)
XLA Ops:
  13.1 2.4 scatter_custom_fusion
  17.1 6.0 %gather_fusion = bf16[1024,2048]{1,0:T(8,128)(2,1)} fusion(bf16[256,2048]{1,0:T(8,128)(2,1)S(1)} %fusion.37, s32[1024]{0:T(1024)S(1)} %fusion.46), kind=kCustom, calls=%fused_computation | custom fusion | bytes 8392704 | tf_op jit(solution)/shard_map/gather | solution.py:114
  24.5 32.9 %all_to_all.10 = bf16[8,128,512]{2,1,0:T(8,128)(2,1)} all-to-all(bf16[8,128,512]{2,1,0:T(8,128)(2,1)S(1)} %constant_dynamic-slice_fusion), channel_id=1, replica_groups=mesh['ep'=8,'tp'=4] {'ep'}, dimensions={0} | all-to-all | bytes 2097152 | tf_op jit(solution)/shard_map/all_to_all | solution.py:120
  59.0 32.1 %all-gather.11.cloned.1.call-done = bf16[8,128,2048]{2,1,0:T(8,128)(2,1)} async-done(((bf16[8,128,512]{2,1,0:T(8,128)(2,1)}), bf16[8,128,2048]{2,1,0:T(8,128)(2,1)}) %all-gather.11.cloned.1.call-update) | async-done | bytes 4194320 | tf_op jit(solution)/shard_map/all_gather | solution.py:121
  91.1 7.7 %fusion.26 = f32[1024,1024]{1,0:T(8,128)S(1)} fusion(bf16[1024,2048]{1,0:T(8,128)(2,1)} %bitcast.115, bf16[1,2048,1024]{2,1,0:T(8,128)(2,1)} %param.30), kind=kOutput, calls=%fused_computation.30 | convolution fusion | flops 4294967296 | bytes 12582912 | tf_op jit(solution)/shard_map/dot_general | solution.py:124
  98.8 5.4 %multiply_convert_fusion = bf16[1024,1024]{1,0:T(8,128)(2,1)S(1)} fusion(f32[1024,1024]{1,0:T(8,128)S(1)} %fusion.26, bf16[1024,2048]{1,0:T(8,128)(2,1)S(1)} %bitcast.116, bf16[1,2048,1024]{2,1,0:T(8,128)(2,1)S(1)} %copy-done.11), kind=kOutput, calls=%fused_computation.34 | convolution fusion | flops 4301258752 | bytes 14680064 | tf_op jit(solution)/shard_map/dot_general | solution.py:123
  104.2 6.1 %fusion.30 = bf16[8,128,2048]{2,1,0:T(8,128)(2,1)} fusion(bf16[8,128,1024]{2,1,0:T(8,128)(2,1)S(1)} %bitcast.117, bf16[1,1024,2048]{2,1,0:T(8,128)(2,1)S(1)} %copy-done.12), kind=kOutput, calls=%fused_computation.35 | convolution fusion | flops 4297064448 | bytes 10485760 | tf_op jit(solution)/shard_map/dot_general | solution.py:126
  112.0 30.3 %all-gather.5.cloned.1.call-done = bf16[2048,512]{1,0:T(8,128)(2,1)} async-done(((bf16[256,512]{1,0:T(8,128)(2,1)}), bf16[2048,512]{1,0:T(8,128)(2,1)}) %all-gather.5.cloned.1.call-update) | async-done | bytes 2097168 | tf_op jit(solution)/shard_map/all_gather | solution.py:28
  142.4 8.9 %reshape.193 = bf16[4,512,4,2,64]{4,3,2,1,0:T(2,128)(2,1)} reshape(bf16[2048,512]{1,0:T(8,128)(2,1)} %all-gather.5.cloned.1.call-done) | data formatting | bytes 4194304 | tf_op jit(solution)/shard_map/reshape | solution.py:33
  151.2 10.6 %copy.37 = bf16[4,512,4,2,64]{1,4,3,2,0:T(8,128)(2,1)} copy(bf16[4,512,4,2,64]{4,3,2,1,0:T(2,128)(2,1)} %reshape.193) | data formatting | bytes 4194304
  161.8 30.3 %all-gather.7.cloned.1.call-done = bf16[2048,512]{1,0:T(8,128)(2,1)} async-done(((bf16[256,512]{1,0:T(8,128)(2,1)}), bf16[2048,512]{1,0:T(8,128)(2,1)}) %all-gather.7.cloned.1.call-update) | async-done | bytes 2097168 | tf_op jit(solution)/shard_map/all_gather | solution.py:29
  192.2 4.0 %reshape.160 = bf16[4,512,4,128]{3,2,1,0:T(4,128)(2,1)} reshape(bf16[2048,512]{1,0:T(8,128)(2,1)} %all-gather.7.cloned.1.call-done) | data formatting | bytes 4194304 | tf_op jit(solution)/shard_map/reshape | solution.py:34
  196.2 4.4 %copy.38 = bf16[4,512,4,128]{1,3,2,0:T(8,128)(2,1)} copy(bf16[4,512,4,128]{3,2,1,0:T(4,128)(2,1)} %reshape.160) | data formatting | bytes 4194304
  201.2 15.2 %while.15 = (s32[]{:T(128)}, f32[256,4,2]{0,2,1:T(2,128)S(1)}, f32[256,4,2]{0,2,1:T(2,128)S(1)}, f32[256,4,2,128]{0,3,2,1:T(8,128)S(1)}, s32[4]{0:T(128)}, /*ind...) while((s32[]{:T(128)}, f32[256,4,2]{0,2,1:T(2,128)S(1)}, ...), condition=%wide.region_5.6_spmd.clone, body=%wide.region_0.5_spmd.clone.sunk | while | flops 416944896 | bytes 16654685 | solution.py:70
  203.1 7.6 %conditional.3 = ((f32[256,4,2]{0,2,1:T(2,128)S(1)}, f32[256,4,2]{0,2,1:T(2,128)S(1)}, f32[256,4,2,128]{0,3,2,1:T(8,128)S(1)})) conditional(s32[]{:T(128)} %convert_element_type.73, (f32[256,4,2]{0,2,1:T(2,128)S(1)}, f32[256,4,2]{0,2,1:T(2,128)S(1)}, f32[256,4,2,128]{0,3,2,1:T(8,128)S(1)}) %tuple.44, (s32[]{:T(128)}, s32[]{:T(128)}, s32[]{:T(128)}, ...), branch_computations={%region_1.1_spmd, %region_2.4_spmd} | conditional | flops 416944896 | bytes 16653394 | solution.py:66
  205.2 1.9 fusion.2
  208.2 2.5 fusion.11
  218.5 19.1 %reduce-scatter.2.cloned.1.call-done = bf16[8,128,512]{2,1,0:T(8,128)(2,1)} async-done(((bf16[8,128,2048]{2,1,0:T(8,128)(2,1)}), bf16[8,128,512]{2,1,0:T(8,128)(2,1)}) %reduce-scatter.2.cloned.1.call-update) | async-done | bytes 1048592 | tf_op jit(solution)/shard_map/reduce_scatter | solution.py:130
  237.6 6.8 %all-to-all-start.1 = ((bf16[8,128,512]{2,1,0:T(8,128)(2,1)}), bf16[8,128,512]{2,1,0:T(8,128)(2,1)S(1)}, u32[]{:S(2)}, u32[]{:S(2)}) async-start(bf16[8,128,512]{2,1,0:T(8,128)(2,1)} %reduce-scatter.2.cloned.1.call-done), calls=%async_computation.2 | async-start | bytes 2097152 | tf_op jit(solution)/shard_map/all_to_all | solution.py:133
  244.7 11.9 %all-gather.9.cloned.1.call-done = bf16[256,2048]{0,1:T(8,128)(2,1)} async-done(((bf16[256,512]{0,1:T(8,128)(2,1)}), bf16[256,2048]{0,1:T(8,128)(2,1)}) %all-gather.9.cloned.1.call-update) | async-done | bytes 1048592 | tf_op jit(solution)/shard_map/all_gather | solution.py:81
  256.5 2.7 convolution_convert_fusion
  259.2 10.7 %all-to-all-done.1 = bf16[8,128,512]{2,1,0:T(8,128)(2,1)S(1)} async-done(((bf16[8,128,512]{2,1,0:T(8,128)(2,1)}), bf16[8,128,512]{2,1,0:T(8,128)(2,1)S(1)}, u32[]{:S(2)}, u32[]{:S(2)}) %all-to-all-start.1) | async-done | bytes 1048608 | tf_op jit(solution)/shard_map/all_to_all | solution.py:133
  269.9 2.6 gather_fusion.1
  274.2 2.1 multiply_reduce_fusion
  (97 shorter events, 22.6 us)
Async XLA Ops:
  7.2 249.4 %copy-start = (bf16[2048,512]{1,0:T(8,128)(2,1)S(1)}, bf16[2048,512]{1,0:T(8,128)(2,1)}, u32[]{:S(2)}) copy-start(bf16[2048,512]{1,0:T(8,128)(2,1)} %param.23) | copy-start | bytes 6291460
  7.2 83.9 %all-gather.11.cloned.1.call-start = ((), (), s32[]{:S(2)}) async-start(), calls=%async_computation.6 | async-start | bytes 5242880 | tf_op jit(solution)/shard_map/all_gather | solution.py:121
  13.1 2.5 copy-start.7
  57.5 84.9 %all-gather.5.cloned.1.call-start = ((), (), s32[]{:S(2)}) async-start(), calls=%async_computation.3 | async-start | bytes 2359296 | tf_op jit(solution)/shard_map/all_gather | solution.py:28
  58.2 134.0 %all-gather.7.cloned.1.call-start = ((), (), s32[]{:S(2)}) async-start(), calls=%async_computation.4 | async-start | bytes 2359296 | tf_op jit(solution)/shard_map/all_gather | solution.py:29
  58.9 178.6 %reduce-scatter.2.cloned.1.call-start = ((), (), s32[]{:S(2)}) async-start(), calls=%async_computation.7 | async-start | bytes 5242880 | tf_op jit(solution)/shard_map/reduce_scatter | solution.py:130
  91.1 7.7 %copy-start.11 = (bf16[1,2048,1024]{2,1,0:T(8,128)(2,1)S(1)}, bf16[1,2048,1024]{2,1,0:T(8,128)(2,1)}, u32[]{:S(2)}) copy-start(bf16[1,2048,1024]{2,1,0:T(8,128)(2,1)} %param.29) | copy-start | bytes 12582916
  91.1 7.7 %copy-start.13 = (bf16[8,128,2048]{2,1,0:T(8,128)(2,1)S(1)}, bf16[8,128,2048]{2,1,0:T(8,128)(2,1)}, u32[]{:S(2)}) copy-start(bf16[8,128,2048]{2,1,0:T(8,128)(2,1)} %all-gather.11.cloned.1.call-done) | copy-start | bytes 12582916
  98.8 5.4 %copy-start.12 = (bf16[1,1024,2048]{2,1,0:T(8,128)(2,1)S(1)}, bf16[1,1024,2048]{2,1,0:T(8,128)(2,1)}, u32[]{:S(2)}) copy-start(bf16[1,1024,2048]{2,1,0:T(8,128)(2,1)} %param.31) | copy-start | bytes 12582916
  110.3 1.0 copy-start.1
  110.3 1.1 copy-start.9
  110.3 1.1 copy-start.10
  110.3 146.2 %all-gather.9.cloned.1.call-start = ((), (), s32[]{:S(2)}) async-start(), calls=%async_computation.5 | async-start | bytes 1310720 | tf_op jit(solution)/shard_map/all_gather | solution.py:81
  216.4 1.1 copy-start.4
  216.5 1.1 copy-start.5
  216.5 27.9 %copy-start.2 = (f32[256,2]{0,1:T(2,128)S(1)}, f32[256,2]{0,1:T(2,128)}, u32[]{:S(2)}) copy-start(f32[256,2]{0,1:T(2,128)} %param.27) | copy-start | bytes 6148
  216.5 27.9 %copy-start.3 = (f32[256,2]{0,1:T(2,128)S(1)}, f32[256,2]{0,1:T(2,128)}, u32[]{:S(2)}) copy-start(f32[256,2]{0,1:T(2,128)} %param.28) | copy-start | bytes 6148
  216.6 27.9 %copy-start.6 = (s32[256,2]{0,1:T(2,128)S(1)}, s32[256,2]{0,1:T(2,128)}, u32[]{:S(2)}) copy-start(s32[256,2]{0,1:T(2,128)} %get-tuple-element.168) | copy-start | bytes 6148
  216.6 28.0 %copy-start.8 = (s32[512,1]{0,1:T(1,128)S(1)}, s32[512,1]{0,1:T(1,128)}, u32[]{:S(2)}) copy-start(s32[512,1]{0,1:T(1,128)} %copy-done.7) | copy-start | bytes 6148
  237.6 32.3 %all-to-all-start.1 = ((bf16[8,128,512]{2,1,0:T(8,128)(2,1)}), bf16[8,128,512]{2,1,0:T(8,128)(2,1)S(1)}, u32[]{:S(2)}, u32[]{:S(2)}) async-start(bf16[8,128,512]{2,1,0:T(8,128)(2,1)} %reduce-scatter.2.cloned.1.call-done), calls=%async_computation.2 | async-start | bytes 2097152 | tf_op jit(solution)/shard_map/all_to_all | solution.py:133
Sparse Core Ops, SparseCore 0:
  57.6 33.4 all-gather.10
  93.2 49.0 all-gather.4
  144.5 47.6 all-gather.6
  194.6 42.9 reduce-scatter.1
  239.6 16.9 all-gather.8
where the time goes:
time: 284 us; the launch traced here: 283 us
  waiting for transfers between devices  136 us (48%)
  local copies, waits for them, and re-layouts  50.8 us (18%)
  blocking collectives  32.9 us (12%)
  matrix products  26.2 us (9%)
  between operations  14.1 us (5%)
  other arithmetic  11 us (4%)
  starting transfers between devices  7.14 us (3%)
  loops' own time  4.74 us (2%)
    all_to_all x1, blocking collectives, expert_block(): lax.all_to_all(own_columns, 'ep', split_axis=0, concat_axis=0, tiled=True)  32.9 us
    all_gather x1, waiting for transfers between devices, expert_block(): experts_arrived = lax.all_gather(arrived, 'tp', axis=2, tiled=True)  32.1 us
    all_gather x1, waiting for transfers between devices, token_mixer(): value_piece = lax.all_gather(values, 'ep', axis=0, tiled=True)  30.3 us
    all_gather x1, waiting for transfers between devices, token_mixer(): key_piece = lax.all_gather(key_rows, 'ep', axis=0, tiled=True)  30.3 us
    reduce_scatter x1, waiting for transfers between devices, expert_block(): lax.psum_scatter(partial_value.astype(jnp.bfloat16), 'tp', scatter_dimens...  19.1 us
    unnamed x32, local copies, waits for them, and re-layouts  16.7 us
    all_gather x1, waiting for transfers between devices, token_mixer(): lax.all_gather(head_out, 'tp', axis=1, tiled=True)  11.9 us
    all_to_all x1, waiting for transfers between devices, expert_block(): lax.all_to_all(answered, 'ep', split_axis=0, concat_axis=0, tiled=True)  10.7 us
  transfers between devices with their start and end apart: 6, of which 6 were waited for; matrix products, arithmetic and copies ran while one was open for 23% of the time, Pallas kernels for 0%

commit v1 on v0

--- a/solution.py
+++ b/solution.py
@@ -7,6 +7,24 @@
 GROUP_SIZE = 4
 EPSILON = 1e-05
 LOWEST = -1e30
+
+
+def check_lanes(mat, axis_key, in_dim):
+    by_rank = []
+    n = lax.axis_size(axis_key)
+    for it in range(n):
+        by_rank.append((it, (it + 1) % n))
+
+    def define_corner(o_now):
+        if len(o_now) == n:
+            return o_now
+        return define_corner([lax.ppermute(o_now[0], axis_name=axis_key, perm=by_rank), *o_now])
+
+    return jnp.roll(
+        jnp.concatenate(define_corner([mat]), in_dim),
+        (lax.axis_index(axis_key) + 1) * mat.shape[in_dim],
+        in_dim,
+    )
 
 
 def token_mixer(queries, key_rows, values, second_scale, head_gain, out_weight):
@@ -118,7 +136,7 @@
     columns = outgoing.shape[2] // lax.axis_size("tp")
     own_columns = lax.dynamic_slice_in_dim(outgoing, lax.axis_index("tp") * columns, columns, 2)
     arrived = lax.all_to_all(own_columns, "ep", split_axis=0, concat_axis=0, tiled=True)
-    experts_arrived = lax.all_gather(arrived, "tp", axis=2, tiled=True)
+    experts_arrived = check_lanes(arrived, "tp", 2)
     stacked = experts_arrived.reshape(-1, experts_arrived.shape[2])
     gate_act = jnp.dot(stacked, gate_local, preferred_element_type=jnp.float32)
     up_act = jnp.dot(stacked, up_local, preferred_element_type=jnp.float32)

time: 284 us -> 245 us (0.86)
  waiting for transfers between devices: 136 us -> 100 us
  blocking collectives: 32.9 us -> 0 us
  starting transfers between devices: 7.14 us -> 32.7 us
  local copies, waits for them, and re-layouts: 50.8 us -> 57.7 us
  matrix products: 26.2 us -> 22.9 us
    ppermute x0 -> x3, waiting for transfers between devices: none -> 43 us  [define_corner(): lax.ppermute(o_now[0], axis_name=axis_key, perm=by_rank)]
    all_to_all x0 -> x1, waiting for transfers between devices: none -> 33.5 us  [expert_block(): lax.all_to_all(own_columns, 'ep', split_axis=0, concat_axis=0, tiled=True)]
    all_to_all x1 -> x0, blocking collectives: 32.9 us -> none  [expert_block(): lax.all_to_all(own_columns, 'ep', split_axis=0, concat_axis=0, tiled=True)]
    all_gather x1 -> x0, waiting for transfers between devices: 32.1 us -> none  [expert_block(): experts_arrived = lax.all_gather(arrived, 'tp', axis=2, tiled=True)]
    all_gather x1, waiting for transfers between devices: 30.3 us -> 0.01 us  [token_mixer(): value_piece = lax.all_gather(values, 'ep', axis=0, tiled=True)]
    all_gather x1, waiting for transfers between devices: 30.3 us -> 0.01 us  [token_mixer(): key_piece = lax.all_gather(key_rows, 'ep', axis=0, tiled=True)]
    reduce_scatter x1, waiting for transfers between devices: 19.1 us -> 0.41 us  [expert_block(): lax.psum_scatter(partial_value.astype(jnp.bfloat16), 'tp', scatter_dimens...]
    all_to_all x1, starting transfers between devices: 6.76 us -> 25.1 us  [expert_block(): lax.all_to_all(answered, 'ep', split_axis=0, concat_axis=0, tiled=True)]
  transfers between devices with their start and end apart: 6 -> 9, of which waited for: 6 -> 7; matrix products, arithmetic and copies ran while one was open for 23% -> 26% of each run, Pallas kernels for 0% -> 0%
where the time goes in v1:
time: 245 us; the launch traced here: 243 us
  waiting for transfers between devices  100 us (41%)
  local copies, waits for them, and re-layouts  57.7 us (24%)
  starting transfers between devices  32.7 us (13%)
  matrix products  22.9 us (9%)
  between operations  15.9 us (6%)
  other arithmetic  9.59 us (4%)
  loops' own time  4.29 us (2%)
    ppermute x3, waiting for transfers between devices, define_corner(): lax.ppermute(o_now[0], axis_name=axis_key, perm=by_rank)  43 us
    all_to_all x1, waiting for transfers between devices, expert_block(): lax.all_to_all(own_columns, 'ep', split_axis=0, concat_axis=0, tiled=True)  33.5 us
    unnamed x33, local copies, waits for them, and re-layouts  25.6 us
    all_to_all x1, starting transfers between devices, expert_block(): lax.all_to_all(answered, 'ep', split_axis=0, concat_axis=0, tiled=True)  25.1 us
    all_gather x1, waiting for transfers between devices, token_mixer(): lax.all_gather(head_out, 'tp', axis=1, tiled=True)  11.8 us
    all_to_all x1, waiting for transfers between devices, expert_block(): lax.all_to_all(answered, 'ep', split_axis=0, concat_axis=0, tiled=True)  10.6 us
    reshape x1, local copies, waits for them, and re-layouts, token_mixer(): key_blocks = key_piece.reshape(blocks, block_width, local_heads, 2, qk_size)  9.01 us
    all_to_all x1, starting transfers between devices, expert_block(): lax.all_to_all(own_columns, 'ep', split_axis=0, concat_axis=0, tiled=True)  7.28 us
  transfers between devices with their start and end apart: 9, of which 7 were waited for; matrix products, arithmetic and copies ran while one was open for 26% of the time, Pallas kernels for 0%

profile of v1, /device:TPU:0, one launch (start us, length us, event | category | flops | bytes accessed | tf_op | source)
XLA Modules:
  0.0 243.0 jit_solution(12737643492067361521)
XLA Ops:
  11.8 2.4 %scatter_custom_fusion = s32[1024]{0:T(1024)S(1)} fusion(s32[512]{0:T(512)S(1)} %bitcast.114, s32[512]{0:T(512)S(1)} %add_select_fusion, s32[]{:T(128)} %copy.74), kind=kCustom, calls=%fused_computation.85 | custom fusion | bytes 4100 | tf_op jit(solution)/shard_map/scatter | solution.py:131
  17.3 6.0 %gather_fusion = bf16[1024,2048]{1,0:T(8,128)(2,1)} fusion(bf16[256,2048]{1,0:T(8,128)(2,1)S(1)} %fusion.37, s32[1024]{0:T(1024)S(1)} %fusion.46), kind=kCustom, calls=%fused_computation | custom fusion | bytes 8392704 | tf_op jit(solution)/shard_map/gather | solution.py:132
  23.3 2.3 constant_dynamic-slice_fusion.1
  25.6 7.3 %all-to-all-start = ((bf16[8,128,512]{2,1,0:T(8,128)(2,1)}), bf16[8,128,512]{2,1,0:T(8,128)(2,1)S(1)}, u32[]{:S(2)}, u32[]{:S(2)}) async-start(bf16[8,128,512]{2,1,0:T(8,128)(2,1)} %constant_dynamic-slice_fusion.1), calls=%async_computation | async-start | bytes 2097152 | tf_op jit(solution)/shard_map/all_to_all | solution.py:138
  33.7 33.5 %all-to-all-done = bf16[8,128,512]{2,1,0:T(8,128)(2,1)S(1)} async-done(((bf16[8,128,512]{2,1,0:T(8,128)(2,1)}), bf16[8,128,512]{2,1,0:T(8,128)(2,1)S(1)}, u32[]{:S(2)}, u32[]{:S(2)}) %all-to-all-start) | async-done | bytes 1048608 | tf_op jit(solution)/shard_map/all_to_all | solution.py:138
  67.1 14.2 %collective-permute-done = bf16[8,128,512]{2,1,0:T(8,128)(2,1)S(1)} collective-permute-done((bf16[8,128,512]{2,1,0:T(8,128)(2,1)S(1)}, bf16[8,128,512]{2,1,0:T(8,128)(2,1)S(1)}, u32[]{:S(2)}, u32[]{:S(2)}) %collective-permute-start) | collective-permute-done | bytes 1048608 | tf_op jit(solution)/shard_map/ppermute | solution.py:21
  82.4 14.3 %collective-permute-done.1 = bf16[8,128,512]{2,1,0:T(8,128)(2,1)} collective-permute-done((bf16[8,128,512]{2,1,0:T(8,128)(2,1)S(1)}, bf16[8,128,512]{2,1,0:T(8,128)(2,1)}, u32[]{:S(2)}, u32[]{:S(2)}) %collective-permute-start.1) | collective-permute-done | bytes 1048608 | tf_op jit(solution)/shard_map/ppermute | solution.py:21
  96.8 14.4 %collective-permute-done.2 = bf16[8,128,512]{2,1,0:T(8,128)(2,1)} collective-permute-done((bf16[8,128,512]{2,1,0:T(8,128)(2,1)}, bf16[8,128,512]{2,1,0:T(8,128)(2,1)}, u32[]{:S(2)}, u32[]{:S(2)}) %collective-permute-start.2) | collective-permute-done | bytes 1048608 | tf_op jit(solution)/shard_map/ppermute | solution.py:21
  119.7 4.5 %fusion.28 = f32[1024,1024]{1,0:T(8,128)S(1)} fusion(bf16[1024,2048]{1,0:T(8,128)(2,1)S(1)} %bitcast.106, bf16[1,2048,1024]{2,1,0:T(8,128)(2,1)S(1)} %copy-done.8), kind=kOutput, calls=%fused_computation.32 | convolution fusion | flops 4294967296 | bytes 12582912 | tf_op jit(solution)/shard_map/dot_general | solution.py:141
  124.2 5.2 %multiply_convert_fusion = bf16[1024,1024]{1,0:T(8,128)(2,1)S(1)} fusion(f32[1024,1024]{1,0:T(8,128)S(1)} %fusion.28, bf16[1024,2048]{1,0:T(8,128)(2,1)S(1)} %bitcast.107, bf16[1,2048,1024]{2,1,0:T(8,128)(2,1)S(1)} %copy-done.9), kind=kOutput, calls=%fused_computation.34 | convolution fusion | flops 4301258752 | bytes 14680064 | tf_op jit(solution)/shard_map/dot_general | solution.py:142
  129.4 6.1 %fusion.30 = bf16[8,128,2048]{2,1,0:T(8,128)(2,1)} fusion(bf16[8,128,1024]{2,1,0:T(8,128)(2,1)S(1)} %bitcast.117, bf16[1,1024,2048]{2,1,0:T(8,128)(2,1)S(1)} %copy-done.10), kind=kOutput, calls=%fused_computation.35 | convolution fusion | flops 4297064448 | bytes 10485760 | tf_op jit(solution)/shard_map/dot_general | solution.py:144
  136.7 9.0 %reshape.193 = bf16[4,512,4,2,64]{4,3,2,1,0:T(2,128)(2,1)} reshape(bf16[2048,512]{1,0:T(8,128)(2,1)} %all-gather.4.cloned.1.call-done) | data formatting | bytes 4194304 | tf_op jit(solution)/shard_map/reshape | solution.py:51
  145.7 10.7 %copy.37 = bf16[4,512,4,2,64]{1,4,3,2,0:T(8,128)(2,1)} copy(bf16[4,512,4,2,64]{4,3,2,1,0:T(2,128)(2,1)} %reshape.193) | data formatting | bytes 4194304
  156.4 4.0 %reshape.160 = bf16[4,512,4,128]{3,2,1,0:T(4,128)(2,1)} reshape(bf16[2048,512]{1,0:T(8,128)(2,1)} %all-gather.6.cloned.1.call-done) | data formatting | bytes 4194304 | tf_op jit(solution)/shard_map/reshape | solution.py:52
  160.4 4.3 %copy.38 = bf16[4,512,4,128]{1,3,2,0:T(8,128)(2,1)} copy(bf16[4,512,4,128]{3,2,1,0:T(4,128)(2,1)} %reshape.160) | data formatting | bytes 4194304
  164.8 12.3 %while.15 = (s32[]{:T(128)}, f32[256,4,2]{0,2,1:T(2,128)S(1)}, f32[256,4,2]{0,2,1:T(2,128)S(1)}, f32[256,4,2,128]{0,3,2,1:T(8,128)S(1)}, s32[4]{0:T(128)S(1)}, /...) while((s32[]{:T(128)}, f32[256,4,2]{0,2,1:T(2,128)S(1)}, ...), condition=%wide.region_5.6_spmd.clone, body=%wide.region_0.5_spmd.clone.sunk | while | flops 416944896 | bytes 16654677 | solution.py:88
  166.0 7.4 %conditional.3 = ((f32[256,4,2]{0,2,1:T(2,128)S(1)}, f32[256,4,2]{0,2,1:T(2,128)S(1)}, f32[256,4,2,128]{0,3,2,1:T(8,128)S(1)})) conditional(s32[]{:T(128)} %convert_element_type.73, (f32[256,4,2]{0,2,1:T(2,128)S(1)}, f32[256,4,2]{0,2,1:T(2,128)S(1)}, f32[256,4,2,128]{0,3,2,1:T(8,128)S(1)}) %tuple.44, (s32[]{:T(128)}, s32[]{:T(128)}, s32[]{:T(128)}, ...), branch_computations={%region_1.1_spmd, %region_2.4_spmd} | conditional | flops 416944896 | bytes 16653394 | solution.py:84
  170.9 2.5 %fusion.11 = f32[256,4,2,128]{0,3,2,1:T(8,128)S(1)} fusion(f32[4,2,512,256]{3,2,1,0:T(8,128)S(1)} %get-tuple-element.165, f32[256,4,2]{0,2,1:T(2,128)S(1)} %max.2, pred[256,512]{0,1:T(8,128)(4,1)S(1)} %broadcast_compare_fusion, f32[256,4,2,128]{0,3,2,1:T(8,128)S(1)} %get-tuple-element.71, bf16[4,512,4,128]{1,3,2,0:T(8,128)(2,1)} %get-tuple-element.72, ...), kind=kOutput, calls=%fused_computation.12 | convolution fusion | flops 274202624 | bytes 6963204 | tf_op jit(solution)/shard_map/while/body/eval_jaxpr/cond/branch_1_fun/qhmk,khe->qhme/dot_general | solution.py:75
  178.8 25.1 %all-to-all-start.1 = ((bf16[8,128,512]{2,1,0:T(8,128)(2,1)}), bf16[8,128,512]{2,1,0:T(8,128)(2,1)S(1)}, u32[]{:S(2)}, u32[]{:S(2)}) async-start(bf16[8,128,512]{2,1,0:T(8,128)(2,1)} %reduce-scatter.2.cloned.1.call-done), calls=%async_computation.2 | async-start | bytes 2097152 | tf_op jit(solution)/shard_map/all_to_all | solution.py:151
  204.2 11.8 %all-gather.8.cloned.1.call-done = bf16[256,2048]{0,1:T(8,128)(2,1)} async-done(((bf16[256,512]{0,1:T(8,128)(2,1)}), bf16[256,2048]{0,1:T(8,128)(2,1)}) %all-gather.8.cloned.1.call-update) | async-done | bytes 1048592 | tf_op jit(solution)/shard_map/all_gather | solution.py:99
  216.0 2.7 %convolution_convert_fusion = bf16[256,512]{1,0:T(8,128)(2,1)} fusion(bf16[256,2048]{0,1:T(8,128)(2,1)} %all-gather.8.cloned.1.call-done, bf16[2048,512]{1,0:T(8,128)(2,1)S(1)} %copy-done), kind=kOutput, calls=%fused_computation.41 | convolution fusion | flops 537001984 | bytes 3407872 | tf_op jit(solution)/shard_map/dot_general | solution.py:98
  218.6 10.6 %all-to-all-done.1 = bf16[8,128,512]{2,1,0:T(8,128)(2,1)S(1)} async-done(((bf16[8,128,512]{2,1,0:T(8,128)(2,1)}), bf16[8,128,512]{2,1,0:T(8,128)(2,1)S(1)}, u32[]{:S(2)}, u32[]{:S(2)}) %all-to-all-start.1) | async-done | bytes 1048608 | tf_op jit(solution)/shard_map/all_to_all | solution.py:151
  229.2 2.6 %gather_fusion.1 = bf16[512,512]{1,0:T(8,128)(2,1)} fusion(bf16[1024,512]{1,0:T(8,128)(2,1)S(1)} %bitcast.103, s32[1024]{0:T(1024)S(1)} %pad_clamp_fusion), kind=kCustom, calls=%fused_computation.1 | custom fusion | bytes 1050624 | tf_op jit(solution)/shard_map/gather | solution.py:152
  233.6 2.1 multiply_reduce_fusion
  (104 shorter events, 27.4 us)
Async XLA Ops:
  8.0 208.0 %copy-start = (bf16[2048,512]{1,0:T(8,128)(2,1)S(1)}, bf16[2048,512]{1,0:T(8,128)(2,1)}, u32[]{:S(2)}) copy-start(bf16[2048,512]{1,0:T(8,128)(2,1)} %param.23) | copy-start | bytes 6291460
  25.6 41.5 %all-to-all-start = ((bf16[8,128,512]{2,1,0:T(8,128)(2,1)}), bf16[8,128,512]{2,1,0:T(8,128)(2,1)S(1)}, u32[]{:S(2)}, u32[]{:S(2)}) async-start(bf16[8,128,512]{2,1,0:T(8,128)(2,1)} %constant_dynamic-slice_fusion.1), calls=%async_computation | async-start | bytes 2097152 | tf_op jit(solution)/shard_map/all_to_all | solution.py:138
  32.9 103.8 %all-gather.4.cloned.1.call-start = ((), (), s32[]{:S(2)}) async-start(), calls=%async_computation.3 | async-start | bytes 2359296 | tf_op jit(solution)/shard_map/all_gather | solution.py:46
  33.6 122.8 %all-gather.6.cloned.1.call-start = ((), (), s32[]{:S(2)}) async-start(), calls=%async_computation.4 | async-start | bytes 2359296 | tf_op jit(solution)/shard_map/all_gather | solution.py:47
  67.1 14.2 %collective-permute-start = (bf16[8,128,512]{2,1,0:T(8,128)(2,1)S(1)}, bf16[8,128,512]{2,1,0:T(8,128)(2,1)S(1)}, u32[]{:S(2)}, u32[]{:S(2)}) collective-permute-start(bf16[8,128,512]{2,1,0:T(8,128)(2,1)S(1)} %all-to-all-done), channel_id=1, source_target_pairs={{0,1},{1,2},{2,3},{3,0},{4,5},{5,6},{6,7},{7,4},{8,9},{9,10},{10,1... | collective-permute-start | bytes 3145736 | tf_op jit(solution)/shard_map/ppermute | solution.py:21
  81.4 1.0 copy-start.1
  82.4 14.3 %collective-permute-start.1 = (bf16[8,128,512]{2,1,0:T(8,128)(2,1)S(1)}, bf16[8,128,512]{2,1,0:T(8,128)(2,1)}, u32[]{:S(2)}, u32[]{:S(2)}) collective-permute-start(bf16[8,128,512]{2,1,0:T(8,128)(2,1)S(1)} %collective-permute-done), channel_id=1, source_target_pairs={{0,1},{1,2},{2,3},{3,0},{4,5},{5,6},{6,7},{7,4},{8,9},{9,10},{10,1... | collective-permute-start | bytes 3145736 | tf_op jit(solution)/shard_map/ppermute | solution.py:21
  96.7 14.5 %collective-permute-start.2 = (bf16[8,128,512]{2,1,0:T(8,128)(2,1)}, bf16[8,128,512]{2,1,0:T(8,128)(2,1)}, u32[]{:S(2)}, u32[]{:S(2)}) collective-permute-start(bf16[8,128,512]{2,1,0:T(8,128)(2,1)} %collective-permute-done.1), channel_id=1, source_target_pairs={{0,1},{1,2},{2,3},{3,0},{4,5},{5,6},{6,7},{7,4},{8,9},{9,10},{10,1... | collective-permute-start | bytes 3145736 | tf_op jit(solution)/shard_map/ppermute | solution.py:21
  96.8 82.0 %reduce-scatter.2.cloned.1.call-start = ((), (), s32[]{:S(2)}) async-start(), calls=%async_computation.6 | async-start | bytes 5242880 | tf_op jit(solution)/shard_map/reduce_scatter | solution.py:148
  96.8 17.2 %copy-start.2 = (bf16[8,128,512]{2,1,0:T(8,128)(2,1)S(1)}, bf16[8,128,512]{2,1,0:T(8,128)(2,1)}, u32[]{:S(2)}) copy-start(bf16[8,128,512]{2,1,0:T(8,128)(2,1)} %copy-done.1) | copy-start | bytes 3145732
  117.5 2.2 copy-start.8
  119.7 4.5 %copy-start.9 = (bf16[1,2048,1024]{2,1,0:T(8,128)(2,1)S(1)}, bf16[1,2048,1024]{2,1,0:T(8,128)(2,1)}, u32[]{:S(2)}) copy-start(bf16[1,2048,1024]{2,1,0:T(8,128)(2,1)} %param.30) | copy-start | bytes 12582916
  124.2 5.2 %copy-start.10 = (bf16[1,1024,2048]{2,1,0:T(8,128)(2,1)S(1)}, bf16[1,1024,2048]{2,1,0:T(8,128)(2,1)}, u32[]{:S(2)}) copy-start(bf16[1,1024,2048]{2,1,0:T(8,128)(2,1)} %param.31) | copy-start | bytes 12582916
  135.5 0.9 copy-start.3
  135.5 1.1 copy-start.6
  135.5 1.1 copy-start.7
  135.6 80.4 %all-gather.8.cloned.1.call-start = ((), (), s32[]{:S(2)}) async-start(), calls=%async_computation.5 | async-start | bytes 1310720 | tf_op jit(solution)/shard_map/all_gather | solution.py:99
  177.1 26.8 %copy-start.4 = (f32[256,2]{0,1:T(2,128)S(1)}, f32[256,2]{0,1:T(2,128)}, u32[]{:S(2)}) copy-start(f32[256,2]{0,1:T(2,128)} %param.27) | copy-start | bytes 6148
  177.1 26.8 %copy-start.5 = (f32[256,2]{0,1:T(2,128)S(1)}, f32[256,2]{0,1:T(2,128)}, u32[]{:S(2)}) copy-start(f32[256,2]{0,1:T(2,128)} %param.28) | copy-start | bytes 6148
  178.8 50.5 %all-to-all-start.1 = ((bf16[8,128,512]{2,1,0:T(8,128)(2,1)}), bf16[8,128,512]{2,1,0:T(8,128)(2,1)S(1)}, u32[]{:S(2)}, u32[]{:S(2)}) async-start(bf16[8,128,512]{2,1,0:T(8,128)(2,1)} %reduce-scatter.2.cloned.1.call-done), calls=%async_computation.2 | async-start | bytes 2097152 | tf_op jit(solution)/shard_map/all_to_all | solution.py:151
Sparse Core Ops, SparseCore 0:
  35.8 58.0 all-gather.3
  96.9 48.1 all-gather.5
Sparse Core Ops, SparseCore 1:
  135.7 43.1 reduce-scatter.1
  180.8 35.1 all-gather.7
